TPU v7x, 32 devices: a whole 2x2x4 slice. The times are simulated.
32 devices in a mesh: fs: 4 (over z), tp: 4 (over y, x), rep: 2 (over core).
Axes of the slice: x: 2, y: 2, z: 4, core: 2. Of those that a mesh axis runs over, the one named last changes fastest.
Arguments:
- gate_weight: float32 [2048, 5632], P('fs', 'tp'), may hold values from -6 to 6
- gate_momentum: float32 [2048, 5632], P('fs', 'tp'), may hold values from -60 to 60
- gate_grads: float32 [2, 2048, 5632], P('rep', 'fs', 'tp'), may hold values from -3500 to 3500
- gate_rows: float32 [2048], P('fs'), may hold values from 0.3 to 3
- gate_columns: float32 [5632], P('tp'), may hold values from 0.3 to 3
- up_weight: float32 [2048, 5632], P('fs', 'tp'), may hold values from -6 to 6
- up_momentum: float32 [2048, 5632], P('fs', 'tp'), may hold values from -60 to 60
- up_grads: float32 [2, 2048, 5632], P('rep', 'fs', 'tp'), may hold values from -3500 to 3500
- up_rows: float32 [2048], P('fs'), may hold values from 0.3 to 3
- up_columns: float32 [5632], P('tp'), may hold values from 0.3 to 3
- down_weight: float32 [5632, 2048], P('fs', 'tp'), may hold values from -6 to 6
- down_momentum: float32 [5632, 2048], P('fs', 'tp'), may hold values from -60 to 60
- down_grads: float32 [2, 5632, 2048], P('rep', 'fs', 'tp'), may hold values from -3500 to 3500
- down_rows: float32 [5632], P('fs'), may hold values from 0.3 to 3
- down_columns: float32 [2048], P('tp'), may hold values from 0.3 to 3
- mixer_weight: float32 [2048, 2048], P('fs', 'tp'), may hold values from -6 to 6
- mixer_momentum: float32 [2048, 2048], P('fs', 'tp'), may hold values from -60 to 60
- mixer_grads: float32 [2, 2048, 2048], P('rep', 'fs', 'tp'), may hold values from -3500 to 3500
- mixer_rows: float32 [2048], P('fs'), may hold values from 0.3 to 3
- mixer_columns: float32 [2048], P('tp'), may hold values from 0.3 to 3
Outputs:
- gate_weight_next: float32 [2048, 5632], P('fs', 'tp')
- gate_momentum_next: float32 [2048, 5632], P('fs', 'tp')
- gate_rows_next: float32 [2048], P('fs')
- gate_columns_next: float32 [5632], P('tp')
- up_weight_next: float32 [2048, 5632], P('fs', 'tp')
- up_momentum_next: float32 [2048, 5632], P('fs', 'tp')
- up_rows_next: float32 [2048], P('fs')
- up_columns_next: float32 [5632], P('tp')
- down_weight_next: float32 [5632, 2048], P('fs', 'tp')
- down_momentum_next: float32 [5632, 2048], P('fs', 'tp')
- down_rows_next: float32 [5632], P('fs')
- down_columns_next: float32 [2048], P('tp')
- mixer_weight_next: float32 [2048, 2048], P('fs', 'tp')
- mixer_momentum_next: float32 [2048, 2048], P('fs', 'tp')
- mixer_rows_next: float32 [2048], P('fs')
- mixer_columns_next: float32 [2048], P('tp')
All inputs are finite; a program needn't handle non-finite values.
Results may differ from a plain program's by a relative error of at most 0.00002.
Values sent between devices are 32-bit elements; how exact they have to be, the bound alone decides.
A program may use at most 128 MiB of HBM per device.

v0:
```python
import functools
import math

import jax
import jax.numpy as jnp
from jax import lax
from jax.experimental import pallas as pl
from jax.experimental.pallas import tpu as pltpu
from jax.sharding import PartitionSpec as P

momentum_decay = 0.9
moment_decay = 0.95
clip_level = 0.25
step_rate = 0.1
MESH = pl.DeviceIdType.MESH
LANES = 128


def chunk_rows(height):
    return LANES if height % LANES == 0 else height


def fold(x):
    return jnp.sum(x.reshape(x.shape[0] // 8, 8, x.shape[1]), axis=0)


def to_lanes(x):
    rows = x.shape[0]
    if rows < LANES:
        x = jnp.concatenate([x, jnp.zeros((LANES - rows, LANES), x.dtype)], axis=0)
    return jnp.sum(x.T, axis=0, keepdims=True)


def to_rows(x, rows):
    return jnp.broadcast_to(x, (LANES, LANES)).T[:rows]


def gather_kernel(sizes, n_fs, n_tp, *refs):
    n_all = n_fs * n_tp
    ins, refs = refs[:20], refs[20:]
    outs, refs = refs[:20], refs[20:]
    own, refs = refs[:4], refs[4:]
    other, refs = refs[:4], refs[4:]
    row_all, refs = refs[:4], refs[4:]
    column_part, refs = refs[:4], refs[4:]
    column_all, refs = refs[:4], refs[4:]
    share_all, refs = refs[:4], refs[4:]
    row_in, refs = refs[:4], refs[4:]
    column_in, refs = refs[:4], refs[4:]
    (own_sem, other_send, other_recv, momentum_sem, weight_sem, moment_sem,
     row_send, row_recv, column_send, column_recv, share_send, share_recv) = refs
    fs, tp, rep = lax.axis_index("fs"), lax.axis_index("tp"), lax.axis_index("rep")
    me = fs * n_tp + tp
    barrier = pltpu.get_barrier_semaphore()

    def place(d):
        lin = lax.rem(me + d, n_all)
        return {"fs": lax.div(lin, n_tp), "tp": lax.rem(lin, n_tp)}

    pl.semaphore_signal(barrier, inc=1, device_id={"rep": 1 - rep}, device_id_type=MESH)

    @pl.loop(1, n_all)
    def _(d):
        pl.semaphore_signal(barrier, inc=1, device_id=place(d), device_id_type=MESH)

    base = [0]
    for height, width in sizes:
        base.append(base[-1] + height // chunk_rows(height))

    def span(k, c):
        rows = chunk_rows(sizes[k][0])
        return pl.ds(pl.multiple_of(c * rows, rows), rows)

    def load(k, c):
        return pltpu.make_async_copy(
            ins[5 * k + 2].at[0, span(k, c)], own[k].at[span(k, c)], own_sem.at[base[k] + c])

    def send(k, c):
        return pltpu.make_async_remote_copy(
            src_ref=own[k].at[span(k, c)], dst_ref=other[k].at[span(k, c)],
            send_sem=other_send.at[base[k] + c], recv_sem=other_recv.at[base[k] + c],
            device_id={"rep": 1 - rep}, device_id_type=MESH)

    def load_momentum(k, c):
        return pltpu.make_async_copy(
            ins[5 * k + 1].at[span(k, c)], outs[5 * k + 1].at[span(k, c)], momentum_sem.at[base[k] + c])

    def load_weight(k):
        return pltpu.make_async_copy(ins[5 * k], outs[5 * k], weight_sem.at[k])

    def load_moments(k):
        return (pltpu.make_async_copy(ins[5 * k + 3], row_in[k], moment_sem.at[k]),
                pltpu.make_async_copy(ins[5 * k + 4], column_in[k], moment_sem.at[4 + k]))

    def each(k, f):
        @pl.loop(0, base[k + 1] - base[k])
        def _(c):
            f(k, c)

    for k in range(4):
        each(k, lambda k, c: load(k, c).start())
    for k in range(4):
        each(k, lambda k, c: load_momentum(k, c).start())
        for copy in load_moments(k):
            copy.start()
    for k in range(4):
        load_weight(k).start()
    pl.semaphore_wait(barrier, n_all)

    def pass_on(k, c):
        load(k, c).wait()
        send(k, c).start()

    for k in range(4):
        each(k, pass_on)

    def accumulate(k):
        height, width = sizes[k]
        rows, tiles = chunk_rows(height), width // LANES
        column_part[k][...] = jnp.zeros_like(column_part[k])

        @pl.loop(0, height // rows)
        def _(c):
            load_momentum(k, c).wait()
            send(k, c).wait_recv()
            part = jnp.zeros((rows, LANES), jnp.float32)
            for j in range(tiles):
                at = (span(k, c), pl.ds(j * LANES, LANES))
                grad = own[k][at] + other[k][at]
                outs[5 * k + 1][at] = momentum_decay * outs[5 * k + 1][at] + (1.0 - momentum_decay) * grad
                square = grad * grad
                part = part + square
                column_part[k][:, pl.ds(j * LANES, LANES)] += fold(square)
            row_all[k][tp, pl.ds(c, 1)] = to_lanes(part)

        for j in range(tiles):
            column_all[k][fs, pl.ds(j, 1)] = jnp.sum(
                column_part[k][:, pl.ds(j * LANES, LANES)], axis=0, keepdims=True)

    def row_copy(k, d):
        peer = lax.rem(tp + d, n_tp)
        return pltpu.make_async_remote_copy(
            src_ref=row_all[k].at[tp], dst_ref=row_all[k].at[tp],
            send_sem=row_send.at[k, d], recv_sem=row_recv.at[k, d],
            device_id={"tp": peer}, device_id_type=MESH)

    def column_copy(k, d):
        peer = lax.rem(fs + d, n_fs)
        return pltpu.make_async_remote_copy(
            src_ref=column_all[k].at[fs], dst_ref=column_all[k].at[fs],
            send_sem=column_send.at[k, d], recv_sem=column_recv.at[k, d],
            device_id={"fs": peer}, device_id_type=MESH)

    def share_copy(k, d):
        return pltpu.make_async_remote_copy(
            src_ref=share_all[k].at[me], dst_ref=share_all[k].at[me],
            send_sem=share_send.at[k, d], recv_sem=share_recv.at[k, d],
            device_id=place(d), device_id_type=MESH)

    def send_sums(k):
        @pl.loop(1, n_fs)
        def _(d):
            column_copy(k, d).start()

        @pl.loop(1, n_tp)
        def _(d):
            row_copy(k, d).start()

    def moments(k):
        height, width = sizes[k]
        rows, tiles = chunk_rows(height), width // LANES

        @pl.loop(1, n_tp)
        def _(d):
            row_copy(k, d).wait_recv()

        @pl.loop(1, n_fs)
        def _(d):
            column_copy(k, d).wait_recv()

        for copy in load_moments(k):
            copy.wait()
        row_total = jnp.sum(row_all[k][...], axis=0) / (width * n_tp)
        row_next = moment_decay * row_in[k][...] + (1.0 - moment_decay) * row_total
        outs[5 * k + 2][...] = row_next
        column_total = jnp.sum(column_all[k][...], axis=0) / (height * n_fs)
        column_next = moment_decay * column_in[k][...] + (1.0 - moment_decay) * column_total
        outs[5 * k + 3][...] = column_next
        lane = lax.broadcasted_iota(jnp.int32, row_next.shape, 1)
        mass = jnp.sum(jnp.where(lane < rows, row_next, 0.0), axis=0, keepdims=True)

        def step(c, sums):
            inverse = to_rows(1.0 / outs[5 * k + 2][pl.ds(c, 1)], rows)
            new = []
            for j in range(tiles):
                m = outs[5 * k + 1][span(k, c), pl.ds(j * LANES, LANES)]
                new.append(sums[j] + fold(m * m * inverse))
            return tuple(new)

        zero = jnp.zeros((8, LANES), jnp.float32)
        sums = lax.fori_loop(0, height // rows, step, (zero,) * tiles)
        share = zero
        for j in range(tiles):
            share = share + sums[j] / outs[5 * k + 3][pl.ds(j, 1)]
        share = jnp.sum(share, axis=0, keepdims=True)
        share_all[k][me] = jnp.concatenate([share, mass], axis=0)

    def send_share(k):
        @pl.loop(1, n_all)
        def _(d):
            share_copy(k, d).start()

    def scale(k):
        height, width = sizes[k]

        @pl.loop(1, n_all)
        def _(d):
            share_copy(k, d).wait_recv()

        total = jnp.sum(share_all[k][...], axis=0)
        total = jnp.sum(total, axis=1, keepdims=True)
        row_mean = total[1:2] / (height * n_fs * n_tp)
        spread = jnp.sqrt(row_mean * total[0:1] / (height * n_fs * width * n_tp))
        factor = jnp.maximum(1.0, spread / clip_level)
        outs[5 * k + 4][...] = jnp.broadcast_to(step_rate * jnp.sqrt(row_mean) / factor, (1, LANES))

    for k in range(4):
        accumulate(k)
        send_sums(k)
        if k >= 1:
            moments(k - 1)
            send_share(k - 1)
        if k >= 2:
            scale(k - 2)
    moments(3)
    send_share(3)
    scale(2)
    scale(3)
    for k in range(4):
        load_weight(k).wait()
        each(k, lambda k, c: send(k, c).wait_send())

        @pl.loop(1, n_tp)
        def _(d):
            row_copy(k, d).wait_send()

        @pl.loop(1, n_fs)
        def _(d):
            column_copy(k, d).wait_send()

        @pl.loop(1, n_all)
        def _(d):
            share_copy(k, d).wait_send()


def write_kernel(sizes, *refs):
    ins, refs = refs[:20], refs[20:]
    outs, refs = refs[:16], refs[16:]
    weight_next, refs = refs[:4], refs[4:]
    momentum_sem, weight_sem = refs

    def put_momentum(k):
        return pltpu.make_async_copy(ins[5 * k + 1], outs[4 * k + 1], momentum_sem.at[k])

    base = [0]
    for height, width in sizes:
        base.append(base[-1] + height // chunk_rows(height))

    def span(k, c):
        rows = chunk_rows(sizes[k][0])
        return pl.ds(pl.multiple_of(c * rows, rows), rows)

    def put_weight(k, c):
        return pltpu.make_async_copy(
            weight_next[k].at[span(k, c)], outs[4 * k].at[span(k, c)], weight_sem.at[base[k] + c])

    for k in range(4):
        put_momentum(k).start()
    for k, (height, width) in enumerate(sizes):
        rows = chunk_rows(height)
        outs[4 * k + 2][...] = ins[5 * k + 2][:, :rows]
        outs[4 * k + 3][...] = ins[5 * k + 3][...]

        @pl.loop(0, height // rows)
        def _(c):
            row_factor = to_rows(lax.rsqrt(ins[5 * k + 2][pl.ds(c, 1)]), rows)
            for j in range(width // LANES):
                at = (span(k, c), pl.ds(j * LANES, LANES))
                column_factor = lax.rsqrt(ins[5 * k + 3][pl.ds(j, 1)]) * ins[5 * k + 4][...]
                weight_next[k][at] = ins[5 * k][at] - ins[5 * k + 1][at] * row_factor * column_factor
            put_weight(k, c).start()

    for k, (height, width) in enumerate(sizes):
        put_momentum(k).wait()

        @pl.loop(0, height // chunk_rows(height))
        def _(c):
            put_weight(k, c).wait()


def body(n_fs, n_tp, *arrays):
    f32 = jnp.float32
    sizes = tuple(arrays[5 * k].shape for k in range(4))
    chunks = [height // chunk_rows(height) for height, _ in sizes]
    n_all, total = n_fs * n_tp, sum(chunks)
    operands, middle = [], []
    in_specs = []
    hbm, vmem = pl.BlockSpec(memory_space=pl.ANY), pl.BlockSpec(memory_space=pltpu.VMEM)
    for k, (height, width) in enumerate(sizes):
        w, m, g, r, c = arrays[5 * k:5 * k + 5]
        rows = chunk_rows(height)
        r = r.reshape(chunks[k], rows)
        if rows < LANES:
            r = jnp.pad(r, ((0, 0), (0, LANES - rows)), constant_values=1.0)
        c = c.reshape(width // LANES, LANES)
        operands += [pltpu.with_memory_space_constraint(x, pltpu.HBM) for x in (w, m, g, r, c)]
        in_specs += [hbm] * 5
        middle += [pltpu.VMEM((height, width), f32), pltpu.VMEM((height, width), f32),
                   pltpu.VMEM((chunks[k], LANES), f32), pltpu.VMEM((width // LANES, LANES), f32), pltpu.VMEM((1, LANES), f32)]
    scratch = [pltpu.VMEM(s, f32) for s in sizes] + [pltpu.VMEM(s, f32) for s in sizes]
    scratch += [pltpu.VMEM((n_tp, n, LANES), f32) for n in chunks]
    scratch += [pltpu.VMEM((8, s[1]), f32) for s in sizes]
    scratch += [pltpu.VMEM((n_fs, s[1] // LANES, LANES), f32) for s in sizes]
    scratch += [pltpu.VMEM((n_all, 2, LANES), f32) for s in sizes]
    scratch += [pltpu.VMEM((n, LANES), f32) for n in chunks]
    scratch += [pltpu.VMEM((s[1] // LANES, LANES), f32) for s in sizes]
    dma = pltpu.SemaphoreType.DMA
    scratch += [dma((total,)), dma((total,)), dma((total,)), dma((total,)), dma((4,)), dma((8,))]
    scratch += [dma((4, n_tp)), dma((4, n_tp)), dma((4, n_fs)), dma((4, n_fs)), dma((4, n_all)), dma((4, n_all))]
    block = 4 * sum(h * w for h, w in sizes)
    slack = 4 << 20
    middle = pl.pallas_call(
        functools.partial(gather_kernel, sizes, n_fs, n_tp),
        out_shape=middle,
        in_specs=in_specs,
        out_specs=[vmem] * 20,
        scratch_shapes=scratch,
        compiler_params=pltpu.CompilerParams(
            collective_id=0, has_side_effects=True, vmem_limit_bytes=2 * block + slack),
        name="gather",
    )(*operands)
    out_shape, out_specs = [], []
    for k, (height, width) in enumerate(sizes):
        rows = chunk_rows(height)
        out_shape += [jax.ShapeDtypeStruct((height, width), f32)] * 2
        out_shape += [jax.ShapeDtypeStruct((chunks[k], rows), f32), jax.ShapeDtypeStruct((width // LANES, LANES), f32)]
        out_specs += [hbm, hbm, vmem, vmem]
    outs = pl.pallas_call(
        functools.partial(write_kernel, sizes),
        out_shape=out_shape,
        in_specs=[vmem] * 20,
        out_specs=out_specs,
        scratch_shapes=[pltpu.VMEM(s, f32) for s in sizes] + [dma((4,)), dma((total,))],
        compiler_params=pltpu.CompilerParams(vmem_limit_bytes=block + slack),
        name="write",
    )(*middle)
    results = []
    for k in range(4):
        results += [outs[4 * k], outs[4 * k + 1], outs[4 * k + 2].reshape(-1), outs[4 * k + 3].reshape(-1)]
    return tuple(results)


def solution(mesh):
    matrix, partial, row, column = P("fs", "tp"), P("rep", "fs", "tp"), P("fs"), P("tp")
    return jax.shard_map(
        functools.partial(body, mesh.shape["fs"], mesh.shape["tp"]),
        mesh=mesh,
        in_specs=(matrix, matrix, partial, row, column) * 4,
        out_specs=(matrix, matrix, row, column) * 4,
        check_vma=False,
    )
```

profile of v0, /device:TPU:0, one launch (start us, length us, event | category | flops | bytes accessed | tf_op | source)
XLA Modules:
  0.0 41.8 jit_solution(16961321550148199342)
XLA Ops:
  0.7 33.6 %gather.1 = (f32[512,1408]{1,0:T(8,128)S(1)}, f32[512,1408]{1,0:T(8,128)S(1)}, f32[4,128]{1,0:T(4,128)S(1)}, f32[11,128]{1,0:T(8,128)S(1)}, f32[1,128]{1,0:T(1,1...) custom-call(f32[512,1408]{1,0:T(8,128)} %refs_0_.1, ...), custom_call_target="tpu_custom_call" | custom-call | tf_op jit(solution)/shard_map/gather/pallas_call | solution.py:332
  34.2 7.5 %write.1 = (f32[512,1408]{1,0:T(8,128)}, f32[512,1408]{1,0:T(8,128)}, f32[4,128]{1,0:T(4,128)}, f32[11,128]{1,0:T(8,128)}, f32[512,1408]{1,0:T(8,128)}, /*index=...) custom-call(f32[512,1408]{1,0:T(8,128)S(1)} %get-tuple-element.52.re, ...), custom_call_target="tpu_custom_call" | custom-call | tf_op jit(solution)/shard_map/write/pallas_call | solution.py:348
where the time goes:
time: 41.9 us; the launch traced here: 41.8 us
  Pallas kernels  41.1 us (98%)
  between operations  0.66 us (2%)
    pallas_call x1, Pallas kernels, body(): pl.pallas_call(functools.partial(gather_kernel, sizes, n_fs, n_tp), out_s...  33.6 us
    pallas_call x1, Pallas kernels, body(): pl.pallas_call(functools.partial(write_kernel, sizes), out_shape=out_shap...  7.53 us

commit v1 on v0

v1 whole, which is shorter than its diff:
```python
import functools

import jax
import jax.numpy as jnp
from jax import lax
from jax.experimental import pallas as pl
from jax.experimental.pallas import tpu as pltpu
from jax.sharding import PartitionSpec as P

momentum_decay = 0.9
moment_decay = 0.95
clip_level = 0.25
step_rate = 0.1
MESH = pl.DeviceIdType.MESH
LANES = 128


class Plan:
    def __init__(self, height, width):
        rows = LANES if height % LANES == 0 else height
        tiles = width // LANES
        if (height // rows) % 2 and tiles % 2:
            rows //= 2
        self.height, self.width, self.rows, self.tiles = height, width, rows, tiles
        self.chunks = height // rows
        self.by_rows = self.chunks % 2 == 0
        self.own_chunks = self.chunks // 2 if self.by_rows else self.chunks
        self.own_tiles = tiles if self.by_rows else tiles // 2
        self.region = (self.own_chunks * rows, self.own_tiles * LANES)

    def row_at(self, owner, c):
        start = (owner * self.own_chunks + c) * self.rows if self.by_rows else c * self.rows
        return pl.multiple_of(start, self.rows)

    def column_at(self, owner, j=0):
        return j * LANES if self.by_rows else pl.multiple_of((owner * self.own_tiles + j) * LANES, LANES)

    def chunk(self, owner, c):
        return pl.ds(self.row_at(owner, c), self.rows), pl.ds(self.column_at(owner), self.region[1])

    def block(self, owner):
        return pl.ds(self.row_at(owner, 0), self.region[0]), pl.ds(self.column_at(owner), self.region[1])

    def tile(self, owner, c, j):
        return pl.ds(self.row_at(owner, c), self.rows), pl.ds(self.column_at(owner, j), LANES)


def fold(x):
    return jnp.sum(x.reshape(x.shape[0] // 8, 8, x.shape[1]), axis=0)


def to_lanes(x):
    rows = x.shape[0]
    if rows < LANES:
        x = jnp.concatenate([x, jnp.zeros((LANES - rows, LANES), x.dtype)], axis=0)
    return jnp.sum(x.T, axis=0, keepdims=True)


def to_rows(x, rows):
    return jnp.broadcast_to(x, (LANES, LANES)).T[:rows]


def gather_kernel(plans, n_fs, n_tp, *refs):
    n_all = n_fs * n_tp
    ins, refs = refs[:20], refs[20:]
    outs, refs = refs[:20], refs[20:]
    own, refs = refs[:4], refs[4:]
    other, refs = refs[:4], refs[4:]
    row_all, refs = refs[:4], refs[4:]
    column_part, refs = refs[:4], refs[4:]
    column_all, refs = refs[:4], refs[4:]
    row_in, refs = refs[:4], refs[4:]
    column_in, refs = refs[:4], refs[4:]
    (share_all, own_sem, other_send, other_recv, momentum_sem, back_send, back_recv, weight_sem, moment_sem,
     row_send, row_recv, column_send, column_recv, share_send, share_recv, ready, everyone) = refs
    fs, tp, rep = lax.axis_index("fs"), lax.axis_index("tp"), lax.axis_index("rep")
    partner = {"rep": 1 - rep}
    barrier = pltpu.get_barrier_semaphore()

    base = [0]
    for p in plans:
        base.append(base[-1] + p.own_chunks)

    def rows_of(p, c):
        return pl.ds(pl.multiple_of(c * p.rows, p.rows), p.rows)

    def load(k, c):
        p = plans[k]
        r, w = p.chunk(rep, c)
        return pltpu.make_async_copy(ins[5 * k + 2].at[0, r, w], own[k].at[rows_of(p, c)], own_sem.at[base[k] + c])

    def load_momentum(k, c):
        at = plans[k].chunk(rep, c)
        return pltpu.make_async_copy(ins[5 * k + 1].at[at], outs[5 * k + 1].at[at], momentum_sem.at[base[k] + c])

    def send(k, c):
        p = plans[k]
        r, w = p.chunk(1 - rep, c)
        return pltpu.make_async_remote_copy(
            src_ref=ins[5 * k + 2].at[0, r, w], dst_ref=other[k].at[rows_of(p, c)],
            send_sem=other_send.at[base[k] + c], recv_sem=other_recv.at[base[k] + c],
            device_id=partner, device_id_type=MESH)

    def give_back(k, owner):
        at = plans[k].block(owner)
        return pltpu.make_async_remote_copy(
            src_ref=outs[5 * k + 1].at[at], dst_ref=outs[5 * k + 1].at[at],
            send_sem=back_send.at[k], recv_sem=back_recv.at[k],
            device_id=partner, device_id_type=MESH)

    def load_weight(k):
        return pltpu.make_async_copy(ins[5 * k], outs[5 * k], weight_sem.at[k])

    def load_moments(k):
        return (pltpu.make_async_copy(ins[5 * k + 3], row_in[k], moment_sem.at[k]),
                pltpu.make_async_copy(ins[5 * k + 4], column_in[k], moment_sem.at[4 + k]))

    def each(k, f):
        @pl.loop(0, plans[k].own_chunks)
        def _(c):
            f(k, c)

    def place(d):
        lin = lax.rem(fs * n_tp + tp + d, n_all)
        return {"fs": lax.div(lin, n_tp), "tp": lax.rem(lin, n_tp)}

    @pl.when(rep == 1)
    def _():
        pl.semaphore_signal(barrier, inc=1, device_id={"rep": 0}, device_id_type=MESH)

    @pl.when(rep == 0)
    def _():
        pl.semaphore_wait(barrier, 1)
        pl.semaphore_signal(ready, inc=1, device_id={"rep": 1}, device_id_type=MESH)

    @pl.when(rep == 1)
    def _():
        pl.semaphore_wait(ready, 1)

    for k in range(4):
        each(k, lambda k, c: send(k, c).start())

    @pl.when(rep == 1)
    def _():
        @pl.loop(1, n_all)
        def _(d):
            pl.semaphore_signal(barrier, inc=1, device_id=place(d), device_id_type=MESH)

    for k in range(4):
        each(k, lambda k, c: load(k, c).start())
        each(k, lambda k, c: load_momentum(k, c).start())
    for k in range(4):
        for copy in load_moments(k):
            copy.start()
    for k in range(4):
        load_weight(k).start()

    def accumulate(k):
        p = plans[k]
        column_part[k][...] = jnp.zeros_like(column_part[k])

        @pl.loop(0, p.own_chunks)
        def _(c):
            load(k, c).wait()
            load_momentum(k, c).wait()
            send(k, c).wait_recv()
            part = jnp.zeros((p.rows, LANES), jnp.float32)
            for j in range(p.own_tiles):
                at = (rows_of(p, c), pl.ds(j * LANES, LANES))
                full = p.tile(rep, c, j)
                grad = own[k][at] + other[k][at]
                outs[5 * k + 1][full] = momentum_decay * outs[5 * k + 1][full] + (1.0 - momentum_decay) * grad
                square = grad * grad
                part = part + square
                column_part[k][:, pl.ds(j * LANES, LANES)] += fold(square)
            row_all[k][rep, tp, pl.ds(c, 1)] = to_lanes(part)

        for j in range(p.own_tiles):
            column_all[k][rep, fs, pl.ds(j, 1)] = jnp.sum(
                column_part[k][:, pl.ds(j * LANES, LANES)], axis=0, keepdims=True)

    def row_copy(k, d):
        lin = lax.rem(rep * n_tp + tp + d, 2 * n_tp)
        return pltpu.make_async_remote_copy(
            src_ref=row_all[k].at[rep, tp], dst_ref=row_all[k].at[rep, tp],
            send_sem=row_send.at[k, d], recv_sem=row_recv.at[k, d],
            device_id={"rep": lax.div(lin, n_tp), "tp": lax.rem(lin, n_tp)}, device_id_type=MESH)

    def column_copy(k, d):
        lin = lax.rem(rep * n_fs + fs + d, 2 * n_fs)
        return pltpu.make_async_remote_copy(
            src_ref=column_all[k].at[rep, fs], dst_ref=column_all[k].at[rep, fs],
            send_sem=column_send.at[k, d], recv_sem=column_recv.at[k, d],
            device_id={"rep": lax.div(lin, n_fs), "fs": lax.rem(lin, n_fs)}, device_id_type=MESH)

    me = (rep * n_fs + fs) * n_tp + tp

    def share_copy(d):
        lin = lax.rem(me + d, 2 * n_all)
        at = lax.rem(lin, n_all)
        return pltpu.make_async_remote_copy(
            src_ref=share_all.at[me], dst_ref=share_all.at[me],
            send_sem=share_send.at[d], recv_sem=share_recv.at[d],
            device_id={"rep": lax.div(lin, n_all), "fs": lax.div(at, n_tp), "tp": lax.rem(at, n_tp)},
            device_id_type=MESH)

    def moments(k):
        p = plans[k]

        @pl.loop(1, 2 * n_tp)
        def _(d):
            row_copy(k, d).wait_recv()

        @pl.loop(1, 2 * n_fs)
        def _(d):
            column_copy(k, d).wait_recv()

        for copy in load_moments(k):
            copy.wait()
        row_sums = [jnp.sum(row_all[k][q], axis=0) for q in range(2)]
        column_sums = [jnp.sum(column_all[k][q], axis=0) for q in range(2)]
        row_scale = (1.0 - moment_decay) / (p.width * n_tp)
        column_scale = (1.0 - moment_decay) / (p.height * n_fs)
        if p.by_rows:
            for q in range(2):
                at = pl.ds(q * p.own_chunks, p.own_chunks)
                outs[5 * k + 2][at] = moment_decay * row_in[k][at] + row_scale * row_sums[q]
            outs[5 * k + 3][...] = moment_decay * column_in[k][...] + column_scale * (column_sums[0] + column_sums[1])
            mine = outs[5 * k + 2][pl.ds(rep * p.own_chunks, p.own_chunks)]
        else:
            outs[5 * k + 2][...] = moment_decay * row_in[k][...] + row_scale * (row_sums[0] + row_sums[1])
            for q in range(2):
                at = pl.ds(q * p.own_tiles, p.own_tiles)
                outs[5 * k + 3][at] = moment_decay * column_in[k][at] + column_scale * column_sums[q]
            mine = outs[5 * k + 2][...]
        lane = lax.broadcasted_iota(jnp.int32, mine.shape, 1)
        mass = jnp.sum(jnp.where(lane < p.rows, mine, 0.0), axis=0, keepdims=True)
        first_chunk = rep * p.own_chunks if p.by_rows else 0
        first_tile = 0 if p.by_rows else rep * p.own_tiles

        def step(c, sums):
            inverse = to_rows(1.0 / outs[5 * k + 2][pl.ds(first_chunk + c, 1)], p.rows)
            new = []
            for j in range(p.own_tiles):
                m = outs[5 * k + 1][p.tile(rep, c, j)]
                new.append(sums[j] + fold(m * m * inverse))
            return tuple(new)

        zero = jnp.zeros((8, LANES), jnp.float32)
        sums = lax.fori_loop(0, p.own_chunks, step, (zero,) * p.own_tiles)
        share = zero
        for j in range(p.own_tiles):
            share = share + sums[j] / outs[5 * k + 3][pl.ds(first_tile + j, 1)]
        share_all[me, pl.ds(2 * k, 1)] = jnp.sum(share, axis=0, keepdims=True)
        share_all[me, pl.ds(2 * k + 1, 1)] = mass

    for k in range(4):
        accumulate(k)
        if k == 0:
            @pl.when(rep == 1)
            def _():
                pl.semaphore_wait(barrier, n_all - 1)
                pl.semaphore_signal(everyone, inc=1, device_id={"rep": 0}, device_id_type=MESH)

            @pl.when(rep == 0)
            def _():
                pl.semaphore_wait(everyone, 1)

        @pl.loop(1, 2 * n_fs)
        def _(d):
            column_copy(k, d).start()

        @pl.loop(1, 2 * n_tp)
        def _(d):
            row_copy(k, d).start()

    for k in range(4):
        give_back(k, rep).start()
    for k in range(4):
        moments(k)

    @pl.loop(1, 2 * n_all)
    def _(d):
        share_copy(d).start()

    @pl.loop(1, 2 * n_all)
    def _(d):
        share_copy(d).wait_recv()

    total = jnp.sum(jnp.sum(share_all[...], axis=0), axis=1, keepdims=True)
    for k, p in enumerate(plans):
        copies = n_tp if p.by_rows else 2 * n_tp
        row_mean = total[2 * k + 1:2 * k + 2] / (p.height * n_fs * copies)
        spread = jnp.sqrt(row_mean * total[2 * k:2 * k + 1] / (p.height * n_fs * p.width * n_tp))
        factor = jnp.maximum(1.0, spread / clip_level)
        outs[5 * k + 4][...] = jnp.broadcast_to(step_rate * jnp.sqrt(row_mean) / factor, (1, LANES))

    for k in range(4):
        load_weight(k).wait()
        give_back(k, 1 - rep).wait_recv()
        give_back(k, rep).wait_send()
        each(k, lambda k, c: send(k, c).wait_send())

        @pl.loop(1, 2 * n_tp)
        def _(d):
            row_copy(k, d).wait_send()

        @pl.loop(1, 2 * n_fs)
        def _(d):
            column_copy(k, d).wait_send()

    @pl.loop(1, 2 * n_all)
    def _(d):
        share_copy(d).wait_send()


def write_kernel(plans, *refs):
    ins, refs = refs[:20], refs[20:]
    outs, refs = refs[:16], refs[16:]
    weight_next, refs = refs[:4], refs[4:]
    momentum_sem, weight_sem = refs

    def put_momentum(k):
        return pltpu.make_async_copy(ins[5 * k + 1], outs[4 * k + 1], momentum_sem.at[k])

    base = [0]
    for p in plans:
        base.append(base[-1] + p.chunks)

    def span(p, c):
        return pl.ds(pl.multiple_of(c * p.rows, p.rows), p.rows)

    def put_weight(k, c):
        return pltpu.make_async_copy(
            weight_next[k].at[span(plans[k], c)], outs[4 * k].at[span(plans[k], c)], weight_sem.at[base[k] + c])

    for k in range(4):
        put_momentum(k).start()
    for k, p in enumerate(plans):
        outs[4 * k + 2][...] = ins[5 * k + 2][:, :p.rows]
        outs[4 * k + 3][...] = ins[5 * k + 3][...]

        @pl.loop(0, p.chunks)
        def _(c):
            row_factor = to_rows(lax.rsqrt(ins[5 * k + 2][pl.ds(c, 1)]), p.rows)
            for j in range(p.tiles):
                at = (span(p, c), pl.ds(j * LANES, LANES))
                column_factor = lax.rsqrt(ins[5 * k + 3][pl.ds(j, 1)]) * ins[5 * k + 4][...]
                weight_next[k][at] = ins[5 * k][at] - ins[5 * k + 1][at] * row_factor * column_factor
            put_weight(k, c).start()

    for k, p in enumerate(plans):
        put_momentum(k).wait()

        @pl.loop(0, p.chunks)
        def _(c):
            put_weight(k, c).wait()


def body(n_fs, n_tp, *arrays):
    f32 = jnp.float32
    plans = tuple(Plan(*arrays[5 * k].shape) for k in range(4))
    n_all, total, own_total = n_fs * n_tp, sum(p.chunks for p in plans), sum(p.own_chunks for p in plans)
    operands, middle = [], []
    in_specs = []
    hbm, vmem = pl.BlockSpec(memory_space=pl.ANY), pl.BlockSpec(memory_space=pltpu.VMEM)
    for k, p in enumerate(plans):
        w, m, g, r, c = arrays[5 * k:5 * k + 5]
        r = r.reshape(p.chunks, p.rows)
        if p.rows < LANES:
            r = jnp.pad(r, ((0, 0), (0, LANES - p.rows)), constant_values=1.0)
        c = c.reshape(p.tiles, LANES)
        operands += [pltpu.with_memory_space_constraint(x, pltpu.HBM) for x in (w, m, g, r, c)]
        in_specs += [hbm] * 5
        full = (p.height, p.width)
        middle += [pltpu.VMEM(full, f32), pltpu.VMEM(full, f32),
                   pltpu.VMEM((p.chunks, LANES), f32), pltpu.VMEM((p.tiles, LANES), f32), pltpu.VMEM((1, LANES), f32)]
    scratch = [pltpu.VMEM(p.region, f32) for p in plans] * 2
    scratch += [pltpu.VMEM((2, n_tp, p.own_chunks, LANES), f32) for p in plans]
    scratch += [pltpu.VMEM((8, p.region[1]), f32) for p in plans]
    scratch += [pltpu.VMEM((2, n_fs, p.own_tiles, LANES), f32) for p in plans]
    scratch += [pltpu.VMEM((p.chunks, LANES), f32) for p in plans]
    scratch += [pltpu.VMEM((p.tiles, LANES), f32) for p in plans]
    scratch += [pltpu.VMEM((2 * n_all, 8, LANES), f32)]
    dma = pltpu.SemaphoreType.DMA
    scratch += [dma((own_total,)), dma((own_total,)), dma((own_total,)), dma((own_total,))]
    scratch += [dma((4,)), dma((4,)), dma((4,)), dma((8,))]
    scratch += [dma((4, 2 * n_tp)), dma((4, 2 * n_tp)), dma((4, 2 * n_fs)), dma((4, 2 * n_fs))]
    scratch += [dma((2 * n_all,)), dma((2 * n_all,))]
    scratch += [pltpu.SemaphoreType.REGULAR, pltpu.SemaphoreType.REGULAR]
    block = 4 * sum(p.height * p.width for p in plans)
    slack = 8 << 20
    middle = pl.pallas_call(
        functools.partial(gather_kernel, plans, n_fs, n_tp),
        out_shape=middle,
        in_specs=in_specs,
        out_specs=[vmem] * 20,
        scratch_shapes=scratch,
        compiler_params=pltpu.CompilerParams(
            collective_id=0, has_side_effects=True, vmem_limit_bytes=block + slack),
        name="gather",
    )(*operands)
    out_shape, out_specs = [], []
    for p in plans:
        out_shape += [jax.ShapeDtypeStruct((p.height, p.width), f32)] * 2
        out_shape += [jax.ShapeDtypeStruct((p.chunks, p.rows), f32), jax.ShapeDtypeStruct((p.tiles, LANES), f32)]
        out_specs += [hbm, hbm, vmem, vmem]
    outs = pl.pallas_call(
        functools.partial(write_kernel, plans),
        out_shape=out_shape,
        in_specs=[vmem] * 20,
        out_specs=out_specs,
        scratch_shapes=[pltpu.VMEM((p.height, p.width), f32) for p in plans] + [dma((4,)), dma((total,))],
        compiler_params=pltpu.CompilerParams(vmem_limit_bytes=block + slack),
        name="write",
    )(*middle)
    results = []
    for k in range(4):
        results += [outs[4 * k], outs[4 * k + 1], outs[4 * k + 2].reshape(-1), outs[4 * k + 3].reshape(-1)]
    return tuple(results)


def solution(mesh):
    matrix, partial, row, column = P("fs", "tp"), P("rep", "fs", "tp"), P("fs"), P("tp")
    return jax.shard_map(
        functools.partial(body, mesh.shape["fs"], mesh.shape["tp"]),
        mesh=mesh,
        in_specs=(matrix, matrix, partial, row, column) * 4,
        out_specs=(matrix, matrix, row, column) * 4,
        check_vma=False,
    )
```

time: 41.9 us -> 33.6 us (0.80)
  Pallas kernels: 41.1 us -> 32.7 us
    pallas_call x2, Pallas kernels: 41.1 us -> 32.7 us  [the longest x1 25.2 us: body(): pl.pallas_call(functools.partial(gather_kernel, plans, n_fs, n_tp), out_s...]
where the time goes in v1:
time: 33.6 us; the launch traced here: 33.4 us
  Pallas kernels  32.7 us (97%)
  between operations  0.66 us (2%)
    pallas_call x1, Pallas kernels, body(): pl.pallas_call(functools.partial(gather_kernel, plans, n_fs, n_tp), out_s...  25.2 us
    pallas_call x1, Pallas kernels, body(): pl.pallas_call(functools.partial(write_kernel, plans), out_shape=out_shap...  7.53 us

profile of v1, /device:TPU:0, one launch (start us, length us, event | category | flops | bytes accessed | tf_op | source)
XLA Modules:
  0.0 33.4 jit_solution(1953854757519933873)
XLA Ops:
  0.7 25.2 %gather.1 = (f32[512,1408]{1,0:T(8,128)S(1)}, f32[512,1408]{1,0:T(8,128)S(1)}, f32[4,128]{1,0:T(4,128)S(1)}, f32[11,128]{1,0:T(8,128)S(1)}, f32[1,128]{1,0:T(1,1...) custom-call(f32[512,1408]{1,0:T(8,128)} %refs_0_.1, ...), custom_call_target="tpu_custom_call" | custom-call | tf_op jit(solution)/shard_map/gather/pallas_call | solution.py:393
  25.9 7.5 %write.1 = (f32[512,1408]{1,0:T(8,128)}, f32[512,1408]{1,0:T(8,128)}, f32[4,128]{1,0:T(4,128)}, f32[11,128]{1,0:T(8,128)}, f32[512,1408]{1,0:T(8,128)}, /*index=...) custom-call(f32[512,1408]{1,0:T(8,128)S(1)} %get-tuple-element.52.re, ...), custom_call_target="tpu_custom_call" | custom-call | tf_op jit(solution)/shard_map/write/pallas_call | solution.py:408

commit v2 on v1

--- a/solution.py
+++ b/solution.py
@@ -77,28 +77,22 @@
     partner = {"rep": 1 - rep}
     barrier = pltpu.get_barrier_semaphore()
 
-    base = [0]
-    for p in plans:
-        base.append(base[-1] + p.own_chunks)
-
     def rows_of(p, c):
         return pl.ds(pl.multiple_of(c * p.rows, p.rows), p.rows)
 
-    def load(k, c):
-        p = plans[k]
-        r, w = p.chunk(rep, c)
-        return pltpu.make_async_copy(ins[5 * k + 2].at[0, r, w], own[k].at[rows_of(p, c)], own_sem.at[base[k] + c])
-
-    def load_momentum(k, c):
-        at = plans[k].chunk(rep, c)
-        return pltpu.make_async_copy(ins[5 * k + 1].at[at], outs[5 * k + 1].at[at], momentum_sem.at[base[k] + c])
-
-    def send(k, c):
-        p = plans[k]
-        r, w = p.chunk(1 - rep, c)
-        return pltpu.make_async_remote_copy(
-            src_ref=ins[5 * k + 2].at[0, r, w], dst_ref=other[k].at[rows_of(p, c)],
-            send_sem=other_send.at[base[k] + c], recv_sem=other_recv.at[base[k] + c],
+    def load(k):
+        r, w = plans[k].block(rep)
+        return pltpu.make_async_copy(ins[5 * k + 2].at[0, r, w], own[k], own_sem.at[k])
+
+    def load_momentum(k):
+        at = plans[k].block(rep)
+        return pltpu.make_async_copy(ins[5 * k + 1].at[at], outs[5 * k + 1].at[at], momentum_sem.at[k])
+
+    def send(k):
+        r, w = plans[k].block(1 - rep)
+        return pltpu.make_async_remote_copy(
+            src_ref=ins[5 * k + 2].at[0, r, w], dst_ref=other[k],
+            send_sem=other_send.at[k], recv_sem=other_recv.at[k],
             device_id=partner, device_id_type=MESH)
 
     def give_back(k, owner):
@@ -115,10 +109,9 @@
         return (pltpu.make_async_copy(ins[5 * k + 3], row_in[k], moment_sem.at[k]),
                 pltpu.make_async_copy(ins[5 * k + 4], column_in[k], moment_sem.at[4 + k]))
 
-    def each(k, f):
-        @pl.loop(0, plans[k].own_chunks)
-        def _(c):
-            f(k, c)
+    def wait_for(slots, n, sem):
+        some = slots.at[pl.ds(0, n)]
+        pltpu.make_async_copy(some, some, sem).wait()
 
     def place(d):
         lin = lax.rem(fs * n_tp + tp + d, n_all)
@@ -138,7 +131,7 @@
         pl.semaphore_wait(ready, 1)
 
     for k in range(4):
-        each(k, lambda k, c: send(k, c).start())
+        send(k).start()
 
     @pl.when(rep == 1)
     def _():
@@ -147,23 +140,21 @@
             pl.semaphore_signal(barrier, inc=1, device_id=place(d), device_id_type=MESH)
 
     for k in range(4):
-        each(k, lambda k, c: load(k, c).start())
-        each(k, lambda k, c: load_momentum(k, c).start())
+        load(k).start()
+        load_momentum(k).start()
     for k in range(4):
         for copy in load_moments(k):
             copy.start()
-    for k in range(4):
-        load_weight(k).start()
 
     def accumulate(k):
         p = plans[k]
         column_part[k][...] = jnp.zeros_like(column_part[k])
+        load(k).wait()
+        load_momentum(k).wait()
+        send(k).wait_recv()
 
         @pl.loop(0, p.own_chunks)
         def _(c):
-            load(k, c).wait()
-            load_momentum(k, c).wait()
-            send(k, c).wait_recv()
             part = jnp.zeros((p.rows, LANES), jnp.float32)
             for j in range(p.own_tiles):
                 at = (rows_of(p, c), pl.ds(j * LANES, LANES))
@@ -173,24 +164,24 @@
                 square = grad * grad
                 part = part + square
                 column_part[k][:, pl.ds(j * LANES, LANES)] += fold(square)
-            row_all[k][rep, tp, pl.ds(c, 1)] = to_lanes(part)
+            row_all[k][rep * n_tp + tp, pl.ds(c, 1)] = to_lanes(part)
 
         for j in range(p.own_tiles):
-            column_all[k][rep, fs, pl.ds(j, 1)] = jnp.sum(
+            column_all[k][rep * n_fs + fs, pl.ds(j, 1)] = jnp.sum(
                 column_part[k][:, pl.ds(j * LANES, LANES)], axis=0, keepdims=True)
 
     def row_copy(k, d):
         lin = lax.rem(rep * n_tp + tp + d, 2 * n_tp)
         return pltpu.make_async_remote_copy(
-            src_ref=row_all[k].at[rep, tp], dst_ref=row_all[k].at[rep, tp],
-            send_sem=row_send.at[k, d], recv_sem=row_recv.at[k, d],
+            src_ref=row_all[k].at[rep * n_tp + tp], dst_ref=row_all[k].at[rep * n_tp + tp],
+            send_sem=row_send.at[k], recv_sem=row_recv.at[k],
             device_id={"rep": lax.div(lin, n_tp), "tp": lax.rem(lin, n_tp)}, device_id_type=MESH)
 
     def column_copy(k, d):
         lin = lax.rem(rep * n_fs + fs + d, 2 * n_fs)
         return pltpu.make_async_remote_copy(
-            src_ref=column_all[k].at[rep, fs], dst_ref=column_all[k].at[rep, fs],
-            send_sem=column_send.at[k, d], recv_sem=column_recv.at[k, d],
+            src_ref=column_all[k].at[rep * n_fs + fs], dst_ref=column_all[k].at[rep * n_fs + fs],
+            send_sem=column_send.at[k], recv_sem=column_recv.at[k],
             device_id={"rep": lax.div(lin, n_fs), "fs": lax.rem(lin, n_fs)}, device_id_type=MESH)
 
     me = (rep * n_fs + fs) * n_tp + tp
@@ -200,25 +191,19 @@
         at = lax.rem(lin, n_all)
         return pltpu.make_async_remote_copy(
             src_ref=share_all.at[me], dst_ref=share_all.at[me],
-            send_sem=share_send.at[d], recv_sem=share_recv.at[d],
+            send_sem=share_send, recv_sem=share_recv,
             device_id={"rep": lax.div(lin, n_all), "fs": lax.div(at, n_tp), "tp": lax.rem(at, n_tp)},
             device_id_type=MESH)
 
     def moments(k):
         p = plans[k]
 
-        @pl.loop(1, 2 * n_tp)
-        def _(d):
-            row_copy(k, d).wait_recv()
-
-        @pl.loop(1, 2 * n_fs)
-        def _(d):
-            column_copy(k, d).wait_recv()
-
+        wait_for(row_all[k], 2 * n_tp - 1, row_recv.at[k])
+        wait_for(column_all[k], 2 * n_fs - 1, column_recv.at[k])
         for copy in load_moments(k):
             copy.wait()
-        row_sums = [jnp.sum(row_all[k][q], axis=0) for q in range(2)]
-        column_sums = [jnp.sum(column_all[k][q], axis=0) for q in range(2)]
+        row_sums = [jnp.sum(row_all[k][pl.ds(q * n_tp, n_tp)], axis=0) for q in range(2)]
+        column_sums = [jnp.sum(column_all[k][pl.ds(q * n_fs, n_fs)], axis=0) for q in range(2)]
         row_scale = (1.0 - moment_decay) / (p.width * n_tp)
         column_scale = (1.0 - moment_decay) / (p.height * n_fs)
         if p.by_rows:
@@ -277,15 +262,15 @@
     for k in range(4):
         give_back(k, rep).start()
     for k in range(4):
+        load_weight(k).start()
+    for k in range(4):
         moments(k)
 
     @pl.loop(1, 2 * n_all)
     def _(d):
         share_copy(d).start()
 
-    @pl.loop(1, 2 * n_all)
-    def _(d):
-        share_copy(d).wait_recv()
+    wait_for(share_all, 2 * n_all - 1, share_recv)
 
     total = jnp.sum(jnp.sum(share_all[...], axis=0), axis=1, keepdims=True)
     for k, p in enumerate(plans):
@@ -299,19 +284,10 @@
         load_weight(k).wait()
         give_back(k, 1 - rep).wait_recv()
         give_back(k, rep).wait_send()
-        each(k, lambda k, c: send(k, c).wait_send())
-
-        @pl.loop(1, 2 * n_tp)
-        def _(d):
-            row_copy(k, d).wait_send()
-
-        @pl.loop(1, 2 * n_fs)
-        def _(d):
-            column_copy(k, d).wait_send()
-
-    @pl.loop(1, 2 * n_all)
-    def _(d):
-        share_copy(d).wait_send()
+        send(k).wait_send()
+        wait_for(row_all[k], 2 * n_tp - 1, row_send.at[k])
+        wait_for(column_all[k], 2 * n_fs - 1, column_send.at[k])
+    wait_for(share_all, 2 * n_all - 1, share_send)
 
 
 def write_kernel(plans, *refs):
@@ -323,16 +299,12 @@
     def put_momentum(k):
         return pltpu.make_async_copy(ins[5 * k + 1], outs[4 * k + 1], momentum_sem.at[k])
 
-    base = [0]
-    for p in plans:
-        base.append(base[-1] + p.chunks)
-
     def span(p, c):
         return pl.ds(pl.multiple_of(c * p.rows, p.rows), p.rows)
 
     def put_weight(k, c):
         return pltpu.make_async_copy(
-            weight_next[k].at[span(plans[k], c)], outs[4 * k].at[span(plans[k], c)], weight_sem.at[base[k] + c])
+            weight_next[k].at[span(plans[k], c)], outs[4 * k].at[span(plans[k], c)], weight_sem.at[k])
 
     for k in range(4):
         put_momentum(k).start()
@@ -349,18 +321,15 @@
                 weight_next[k][at] = ins[5 * k][at] - ins[5 * k + 1][at] * row_factor * column_factor
             put_weight(k, c).start()
 
-    for k, p in enumerate(plans):
+    for k in range(4):
         put_momentum(k).wait()
-
-        @pl.loop(0, p.chunks)
-        def _(c):
-            put_weight(k, c).wait()
+        pltpu.make_async_copy(weight_next[k], outs[4 * k], weight_sem.at[k]).wait()
 
 
 def body(n_fs, n_tp, *arrays):
     f32 = jnp.float32
     plans = tuple(Plan(*arrays[5 * k].shape) for k in range(4))
-    n_all, total, own_total = n_fs * n_tp, sum(p.chunks for p in plans), sum(p.own_chunks for p in plans)
+    n_all = n_fs * n_tp
     operands, middle = [], []
     in_specs = []
     hbm, vmem = pl.BlockSpec(memory_space=pl.ANY), pl.BlockSpec(memory_space=pltpu.VMEM)
@@ -376,17 +345,14 @@
         middle += [pltpu.VMEM(full, f32), pltpu.VMEM(full, f32),
                    pltpu.VMEM((p.chunks, LANES), f32), pltpu.VMEM((p.tiles, LANES), f32), pltpu.VMEM((1, LANES), f32)]
     scratch = [pltpu.VMEM(p.region, f32) for p in plans] * 2
-    scratch += [pltpu.VMEM((2, n_tp, p.own_chunks, LANES), f32) for p in plans]
+    scratch += [pltpu.VMEM((2 * n_tp, p.own_chunks, LANES), f32) for p in plans]
     scratch += [pltpu.VMEM((8, p.region[1]), f32) for p in plans]
-    scratch += [pltpu.VMEM((2, n_fs, p.own_tiles, LANES), f32) for p in plans]
+    scratch += [pltpu.VMEM((2 * n_fs, p.own_tiles, LANES), f32) for p in plans]
     scratch += [pltpu.VMEM((p.chunks, LANES), f32) for p in plans]
     scratch += [pltpu.VMEM((p.tiles, LANES), f32) for p in plans]
     scratch += [pltpu.VMEM((2 * n_all, 8, LANES), f32)]
     dma = pltpu.SemaphoreType.DMA
-    scratch += [dma((own_total,)), dma((own_total,)), dma((own_total,)), dma((own_total,))]
-    scratch += [dma((4,)), dma((4,)), dma((4,)), dma((8,))]
-    scratch += [dma((4, 2 * n_tp)), dma((4, 2 * n_tp)), dma((4, 2 * n_fs)), dma((4, 2 * n_fs))]
-    scratch += [dma((2 * n_all,)), dma((2 * n_all,))]
+    scratch += [dma((4,))] * 7 + [dma((8,))] + [dma((4,))] * 4 + [dma, dma]
     scratch += [pltpu.SemaphoreType.REGULAR, pltpu.SemaphoreType.REGULAR]
     block = 4 * sum(p.height * p.width for p in plans)
     slack = 8 << 20
@@ -410,7 +376,7 @@
         out_shape=out_shape,
         in_specs=[vmem] * 20,
         out_specs=out_specs,
-        scratch_shapes=[pltpu.VMEM((p.height, p.width), f32) for p in plans] + [dma((4,)), dma((total,))],
+        scratch_shapes=[pltpu.VMEM((p.height, p.width), f32) for p in plans] + [dma((4,)), dma((4,))],
         compiler_params=pltpu.CompilerParams(vmem_limit_bytes=block + slack),
         name="write",
     )(*middle)

time: 33.6 us -> 31.8 us (0.946)
  Pallas kernels: 32.7 us -> 31 us
    pallas_call x1, Pallas kernels: 25.2 us -> 23.6 us  [body(): pl.pallas_call(functools.partial(gather_kernel, plans, n_fs, n_tp), out_s...]
where the time goes in v2:
time: 31.8 us; the launch traced here: 31.6 us
  Pallas kernels  31 us (97%)
  between operations  0.66 us (2%)
    pallas_call x1, Pallas kernels, body(): pl.pallas_call(functools.partial(gather_kernel, plans, n_fs, n_tp), out_s...  23.6 us
    pallas_call x1, Pallas kernels, body(): pl.pallas_call(functools.partial(write_kernel, plans), out_shape=out_shap...  7.36 us

profile of v2, /device:TPU:0, one launch (start us, length us, event | category | flops | bytes accessed | tf_op | source)
XLA Modules:
  0.0 31.6 jit_solution(4883997161260352843)
XLA Ops:
  0.7 23.6 %gather.1 = (f32[512,1408]{1,0:T(8,128)S(1)}, f32[512,1408]{1,0:T(8,128)S(1)}, f32[4,128]{1,0:T(4,128)S(1)}, f32[11,128]{1,0:T(8,128)S(1)}, f32[1,128]{1,0:T(1,1...) custom-call(f32[512,1408]{1,0:T(8,128)} %refs_0_.1, ...), custom_call_target="tpu_custom_call" | custom-call | tf_op jit(solution)/shard_map/gather/pallas_call | solution.py:359
  24.3 7.4 %write.1 = (f32[512,1408]{1,0:T(8,128)}, f32[512,1408]{1,0:T(8,128)}, f32[4,128]{1,0:T(4,128)}, f32[11,128]{1,0:T(8,128)}, f32[512,1408]{1,0:T(8,128)}, /*index=...) custom-call(f32[512,1408]{1,0:T(8,128)S(1)} %get-tuple-element.52.re, ...), custom_call_target="tpu_custom_call" | custom-call | tf_op jit(solution)/shard_map/write/pallas_call | solution.py:374

commit v3 on v2

--- a/solution.py
+++ b/solution.py
@@ -27,6 +27,8 @@
         self.own_chunks = self.chunks // 2 if self.by_rows else self.chunks
         self.own_tiles = tiles if self.by_rows else tiles // 2
         self.region = (self.own_chunks * rows, self.own_tiles * LANES)
+        cut = (self.own_chunks + 1) // 2
+        self.pieces = [(0, cut)] + ([(cut, self.own_chunks)] if cut < self.own_chunks else [])
 
     def row_at(self, owner, c):
         start = (owner * self.own_chunks + c) * self.rows if self.by_rows else c * self.rows
@@ -35,8 +37,8 @@
     def column_at(self, owner, j=0):
         return j * LANES if self.by_rows else pl.multiple_of((owner * self.own_tiles + j) * LANES, LANES)
 
-    def chunk(self, owner, c):
-        return pl.ds(self.row_at(owner, c), self.rows), pl.ds(self.column_at(owner), self.region[1])
+    def part(self, owner, first, last):
+        return pl.ds(self.row_at(owner, first), (last - first) * self.rows), pl.ds(self.column_at(owner), self.region[1])
 
     def block(self, owner):
         return pl.ds(self.row_at(owner, 0), self.region[0]), pl.ds(self.column_at(owner), self.region[1])
@@ -88,11 +90,13 @@
         at = plans[k].block(rep)
         return pltpu.make_async_copy(ins[5 * k + 1].at[at], outs[5 * k + 1].at[at], momentum_sem.at[k])
 
-    def send(k):
-        r, w = plans[k].block(1 - rep)
+    def send(k, i):
+        p = plans[k]
+        first, last = p.pieces[i]
+        r, w = p.part(1 - rep, first, last)
         return pltpu.make_async_remote_copy(
-            src_ref=ins[5 * k + 2].at[0, r, w], dst_ref=other[k],
-            send_sem=other_send.at[k], recv_sem=other_recv.at[k],
+            src_ref=ins[5 * k + 2].at[0, r, w], dst_ref=other[k].at[pl.ds(first * p.rows, (last - first) * p.rows)],
+            send_sem=other_send.at[k], recv_sem=other_recv.at[k, i],
             device_id=partner, device_id_type=MESH)
 
     def give_back(k, owner):
@@ -130,8 +134,9 @@
     def _():
         pl.semaphore_wait(ready, 1)
 
-    for k in range(4):
-        send(k).start()
+    for k, p in enumerate(plans):
+        for i in range(len(p.pieces)):
+            send(k, i).start()
 
     @pl.when(rep == 1)
     def _():
@@ -151,10 +156,8 @@
         column_part[k][...] = jnp.zeros_like(column_part[k])
         load(k).wait()
         load_momentum(k).wait()
-        send(k).wait_recv()
-
-        @pl.loop(0, p.own_chunks)
-        def _(c):
+
+        def step(c):
             part = jnp.zeros((p.rows, LANES), jnp.float32)
             for j in range(p.own_tiles):
                 at = (rows_of(p, c), pl.ds(j * LANES, LANES))
@@ -166,6 +169,10 @@
                 column_part[k][:, pl.ds(j * LANES, LANES)] += fold(square)
             row_all[k][rep * n_tp + tp, pl.ds(c, 1)] = to_lanes(part)
 
+        for i, (first, last) in enumerate(p.pieces):
+            send(k, i).wait_recv()
+            pl.loop(first, last)(step)
+
         for j in range(p.own_tiles):
             column_all[k][rep * n_fs + fs, pl.ds(j, 1)] = jnp.sum(
                 column_part[k][:, pl.ds(j * LANES, LANES)], axis=0, keepdims=True)
@@ -184,15 +191,15 @@
             send_sem=column_send.at[k], recv_sem=column_recv.at[k],
             device_id={"rep": lax.div(lin, n_fs), "fs": lax.rem(lin, n_fs)}, device_id_type=MESH)
 
-    me = (rep * n_fs + fs) * n_tp + tp
+    me = (fs * n_tp + tp) * 2 + rep
 
     def share_copy(d):
         lin = lax.rem(me + d, 2 * n_all)
-        at = lax.rem(lin, n_all)
+        at = lax.div(lin, 2)
         return pltpu.make_async_remote_copy(
             src_ref=share_all.at[me], dst_ref=share_all.at[me],
             send_sem=share_send, recv_sem=share_recv,
-            device_id={"rep": lax.div(lin, n_all), "fs": lax.div(at, n_tp), "tp": lax.rem(at, n_tp)},
+            device_id={"rep": lax.rem(lin, 2), "fs": lax.div(at, n_tp), "tp": lax.rem(at, n_tp)},
             device_id_type=MESH)
 
     def moments(k):
@@ -284,7 +291,7 @@
         load_weight(k).wait()
         give_back(k, 1 - rep).wait_recv()
         give_back(k, rep).wait_send()
-        send(k).wait_send()
+        pltpu.make_async_copy(other[k], other[k], other_send.at[k]).wait()
         wait_for(row_all[k], 2 * n_tp - 1, row_send.at[k])
         wait_for(column_all[k], 2 * n_fs - 1, column_send.at[k])
     wait_for(share_all, 2 * n_all - 1, share_send)
@@ -352,7 +359,7 @@
     scratch += [pltpu.VMEM((p.tiles, LANES), f32) for p in plans]
     scratch += [pltpu.VMEM((2 * n_all, 8, LANES), f32)]
     dma = pltpu.SemaphoreType.DMA
-    scratch += [dma((4,))] * 7 + [dma((8,))] + [dma((4,))] * 4 + [dma, dma]
+    scratch += [dma((4,))] * 2 + [dma((4, 2))] + [dma((4,))] * 4 + [dma((8,))] + [dma((4,))] * 4 + [dma, dma]
     scratch += [pltpu.SemaphoreType.REGULAR, pltpu.SemaphoreType.REGULAR]
     block = 4 * sum(p.height * p.width for p in plans)
     slack = 8 << 20

time: 31.8 us -> 30.3 us (0.953)
  Pallas kernels: 31 us -> 29.5 us
    pallas_call x1, Pallas kernels: 23.6 us -> 22.1 us  [body(): pl.pallas_call(functools.partial(gather_kernel, plans, n_fs, n_tp), out_s...]
where the time goes in v3:
time: 30.3 us; the launch traced here: 30.1 us
  Pallas kernels  29.5 us (97%)
  between operations  0.66 us (2%)
    pallas_call x1, Pallas kernels, body(): pl.pallas_call(functools.partial(gather_kernel, plans, n_fs, n_tp), out_s...  22.1 us
    pallas_call x1, Pallas kernels, body(): pl.pallas_call(functools.partial(write_kernel, plans), out_shape=out_shap...  7.36 us

profile of v3, /device:TPU:0, one launch (start us, length us, event | category | flops | bytes accessed | tf_op | source)
XLA Modules:
  0.0 30.1 jit_solution(4807739892127649141)
XLA Ops:
  0.7 22.1 %gather.1 = (f32[512,1408]{1,0:T(8,128)S(1)}, f32[512,1408]{1,0:T(8,128)S(1)}, f32[4,128]{1,0:T(4,128)S(1)}, f32[11,128]{1,0:T(8,128)S(1)}, f32[1,128]{1,0:T(1,1...) custom-call(f32[512,1408]{1,0:T(8,128)} %refs_0_.1, ...), custom_call_target="tpu_custom_call" | custom-call | tf_op jit(solution)/shard_map/gather/pallas_call | solution.py:366
  22.8 7.4 %write.1 = (f32[512,1408]{1,0:T(8,128)}, f32[512,1408]{1,0:T(8,128)}, f32[4,128]{1,0:T(4,128)}, f32[11,128]{1,0:T(8,128)}, f32[512,1408]{1,0:T(8,128)}, /*index=...) custom-call(f32[512,1408]{1,0:T(8,128)S(1)} %get-tuple-element.52.re, ...), custom_call_target="tpu_custom_call" | custom-call | tf_op jit(solution)/shard_map/write/pallas_call | solution.py:381

commit v4 on v3

--- a/solution.py
+++ b/solution.py
@@ -243,8 +243,8 @@
         share = zero
         for j in range(p.own_tiles):
             share = share + sums[j] / outs[5 * k + 3][pl.ds(first_tile + j, 1)]
-        share_all[me, pl.ds(2 * k, 1)] = jnp.sum(share, axis=0, keepdims=True)
-        share_all[me, pl.ds(2 * k + 1, 1)] = mass
+        share = jnp.sum(jnp.sum(share, axis=0, keepdims=True), axis=1, keepdims=True)
+        return share, jnp.sum(mass, axis=1, keepdims=True)
 
     for k in range(4):
         accumulate(k)
@@ -270,8 +270,12 @@
         give_back(k, rep).start()
     for k in range(4):
         load_weight(k).start()
-    for k in range(4):
-        moments(k)
+    lane = lax.broadcasted_iota(jnp.int32, (1, LANES), 1)
+    packed = jnp.zeros((1, LANES), jnp.float32)
+    for k in range(4):
+        share, mass = moments(k)
+        packed = jnp.where(lane == 2 * k, share, jnp.where(lane == 2 * k + 1, mass, packed))
+    share_all[me] = packed
 
     @pl.loop(1, 2 * n_all)
     def _(d):
@@ -279,11 +283,12 @@
 
     wait_for(share_all, 2 * n_all - 1, share_recv)
 
-    total = jnp.sum(jnp.sum(share_all[...], axis=0), axis=1, keepdims=True)
+    total = jnp.sum(share_all[...], axis=0)
+    totals = [jnp.sum(jnp.where(lane == i, total, 0.0), axis=1, keepdims=True) for i in range(8)]
     for k, p in enumerate(plans):
         copies = n_tp if p.by_rows else 2 * n_tp
-        row_mean = total[2 * k + 1:2 * k + 2] / (p.height * n_fs * copies)
-        spread = jnp.sqrt(row_mean * total[2 * k:2 * k + 1] / (p.height * n_fs * p.width * n_tp))
+        row_mean = totals[2 * k + 1] / (p.height * n_fs * copies)
+        spread = jnp.sqrt(row_mean * totals[2 * k] / (p.height * n_fs * p.width * n_tp))
         factor = jnp.maximum(1.0, spread / clip_level)
         outs[5 * k + 4][...] = jnp.broadcast_to(step_rate * jnp.sqrt(row_mean) / factor, (1, LANES))
 
@@ -357,7 +362,7 @@
     scratch += [pltpu.VMEM((2 * n_fs, p.own_tiles, LANES), f32) for p in plans]
     scratch += [pltpu.VMEM((p.chunks, LANES), f32) for p in plans]
     scratch += [pltpu.VMEM((p.tiles, LANES), f32) for p in plans]
-    scratch += [pltpu.VMEM((2 * n_all, 8, LANES), f32)]
+    scratch += [pltpu.VMEM((2 * n_all, 1, LANES), f32)]
     dma = pltpu.SemaphoreType.DMA
     scratch += [dma((4,))] * 2 + [dma((4, 2))] + [dma((4,))] * 4 + [dma((8,))] + [dma((4,))] * 4 + [dma, dma]
     scratch += [pltpu.SemaphoreType.REGULAR, pltpu.SemaphoreType.REGULAR]

time: 30.3 us -> 29.8 us (0.983)
  Pallas kernels: 29.5 us -> 29 us
    pallas_call x1, Pallas kernels: 22.1 us -> 21.6 us  [body(): pl.pallas_call(functools.partial(gather_kernel, plans, n_fs, n_tp), out_s...]
where the time goes in v4:
time: 29.8 us; the launch traced here: 29.7 us
  Pallas kernels  29 us (97%)
  between operations  0.66 us (2%)
    pallas_call x1, Pallas kernels, body(): pl.pallas_call(functools.partial(gather_kernel, plans, n_fs, n_tp), out_s...  21.6 us
    pallas_call x1, Pallas kernels, body(): pl.pallas_call(functools.partial(write_kernel, plans), out_shape=out_shap...  7.36 us

profile of v4, /device:TPU:0, one launch (start us, length us, event | category | flops | bytes accessed | tf_op | source)
XLA Modules:
  0.0 29.7 jit_solution(17408894254437161779)
XLA Ops:
  0.7 21.6 %gather.1 = (f32[512,1408]{1,0:T(8,128)S(1)}, f32[512,1408]{1,0:T(8,128)S(1)}, f32[4,128]{1,0:T(4,128)S(1)}, f32[11,128]{1,0:T(8,128)S(1)}, f32[1,128]{1,0:T(1,1...) custom-call(f32[512,1408]{1,0:T(8,128)} %refs_0_.1, ...), custom_call_target="tpu_custom_call" | custom-call | tf_op jit(solution)/shard_map/gather/pallas_call | solution.py:371
  22.3 7.4 %write.1 = (f32[512,1408]{1,0:T(8,128)}, f32[512,1408]{1,0:T(8,128)}, f32[4,128]{1,0:T(4,128)}, f32[11,128]{1,0:T(8,128)}, f32[512,1408]{1,0:T(8,128)}, /*index=...) custom-call(f32[512,1408]{1,0:T(8,128)S(1)} %get-tuple-element.52.re, ...), custom_call_target="tpu_custom_call" | custom-call | tf_op jit(solution)/shard_map/write/pallas_call | solution.py:386

commit v5 on v4

--- a/solution.py
+++ b/solution.py
@@ -13,6 +13,7 @@
 step_rate = 0.1
 MESH = pl.DeviceIdType.MESH
 LANES = 128
+ORDER = (2, 0, 1, 3)
 
 
 class Plan:
@@ -134,8 +135,8 @@
     def _():
         pl.semaphore_wait(ready, 1)
 
-    for k, p in enumerate(plans):
-        for i in range(len(p.pieces)):
+    for k in ORDER:
+        for i in range(len(plans[k].pieces)):
             send(k, i).start()
 
     @pl.when(rep == 1)
@@ -144,7 +145,7 @@
         def _(d):
             pl.semaphore_signal(barrier, inc=1, device_id=place(d), device_id_type=MESH)
 
-    for k in range(4):
+    for k in ORDER:
         load(k).start()
         load_momentum(k).start()
     for k in range(4):
@@ -246,9 +247,9 @@
         share = jnp.sum(jnp.sum(share, axis=0, keepdims=True), axis=1, keepdims=True)
         return share, jnp.sum(mass, axis=1, keepdims=True)
 
-    for k in range(4):
+    for k in ORDER:
         accumulate(k)
-        if k == 0:
+        if k == ORDER[0]:
             @pl.when(rep == 1)
             def _():
                 pl.semaphore_wait(barrier, n_all - 1)
@@ -272,7 +273,7 @@
         load_weight(k).start()
     lane = lax.broadcasted_iota(jnp.int32, (1, LANES), 1)
     packed = jnp.zeros((1, LANES), jnp.float32)
-    for k in range(4):
+    for k in ORDER:
         share, mass = moments(k)
         packed = jnp.where(lane == 2 * k, share, jnp.where(lane == 2 * k + 1, mass, packed))
     share_all[me] = packed

time: 29.8 us -> 28.8 us (0.966)
  Pallas kernels: 29 us -> 28 us
    pallas_call x1, Pallas kernels: 21.6 us -> 20.7 us  [body(): pl.pallas_call(functools.partial(gather_kernel, plans, n_fs, n_tp), out_s...]
where the time goes in v5:
time: 28.8 us; the launch traced here: 28.7 us
  Pallas kernels  28 us (97%)
  between operations  0.66 us (2%)
    pallas_call x1, Pallas kernels, body(): pl.pallas_call(functools.partial(gather_kernel, plans, n_fs, n_tp), out_s...  20.7 us
    pallas_call x1, Pallas kernels, body(): pl.pallas_call(functools.partial(write_kernel, plans), out_shape=out_shap...  7.36 us

profile of v5, /device:TPU:0, one launch (start us, length us, event | category | flops | bytes accessed | tf_op | source)
XLA Modules:
  0.0 28.7 jit_solution(5476764161502426931)
XLA Ops:
  0.7 20.7 %gather.1 = (f32[512,1408]{1,0:T(8,128)S(1)}, f32[512,1408]{1,0:T(8,128)S(1)}, f32[4,128]{1,0:T(4,128)S(1)}, f32[11,128]{1,0:T(8,128)S(1)}, f32[1,128]{1,0:T(1,1...) custom-call(f32[512,1408]{1,0:T(8,128)} %refs_0_.1, ...), custom_call_target="tpu_custom_call" | custom-call | tf_op jit(solution)/shard_map/gather/pallas_call | solution.py:372
  21.3 7.4 %write.1 = (f32[512,1408]{1,0:T(8,128)}, f32[512,1408]{1,0:T(8,128)}, f32[4,128]{1,0:T(4,128)}, f32[11,128]{1,0:T(8,128)}, f32[512,1408]{1,0:T(8,128)}, /*index=...) custom-call(f32[512,1408]{1,0:T(8,128)S(1)} %get-tuple-element.52.re, ...), custom_call_target="tpu_custom_call" | custom-call | tf_op jit(solution)/shard_map/write/pallas_call | solution.py:387
